TPU v7x, 512 devices: a whole 4x4x16 slice. The times are simulated.
512 devices in a mesh: sp: 32 (over z, core), tp: 16 (over y, x).
Axes of the slice: x: 4, y: 4, z: 16, core: 2. Of those that a mesh axis runs over, the one named last changes fastest.
Arguments:
- mix_values: bfloat16 [4096, 4096], P('sp', 'tp'), may hold values from -6 to 6
- mix_gate: bfloat16 [4096, 4096], P('sp', 'tp'), may hold values from -6 to 6
- input_keys: bfloat16 [4096, 2048], P('sp', 'tp'), may hold values from -0.22460938 to 0.22460938
- output_keys: bfloat16 [4096, 2048], P('sp', 'tp'), may hold values from -0.22460938 to 0.22460938
- step_sizes: float32 [4096, 64], P('sp', 'tp'), may hold values from 0.1 to 8
- decay_rates: float32 [64], P('tp'), may hold values from 1.2207031e-05 to 0.03
- out_proj: bfloat16 [2048, 4096], P('sp', 'tp'), may hold values from -0.09375 to 0.09375
- expert_inputs: bfloat16 [4096, 2048], P('sp'), may hold values from -20 to 20
- stream_grad: bfloat16 [4096, 2048], P('sp'), may hold values from -6 to 6
- routes: int32 [4096, 2], P('sp'), may hold values from 0 to 31, all different within a row; in each aligned block of 128 rows (0 to 127, 128 to 255, ...) at most 12 rows name the same one
- route_weights: float32 [4096, 2], P('sp'), may hold values from 0.1 to 0.9
- gate_proj: bfloat16 [32, 2048, 2048], P('sp', 'tp'), may hold values from -0.125 to 0.125
- up_proj: bfloat16 [32, 2048, 2048], P('sp', 'tp'), may hold values from -0.125 to 0.125
- down_proj: bfloat16 [32, 2048, 2048], P('sp', 'tp'), may hold values from -0.125 to 0.125
Outputs:
- grad_gate_proj: bfloat16 [32, 2048, 2048], P('sp', 'tp')
- grad_up_proj: bfloat16 [32, 2048, 2048], P('sp', 'tp')
- grad_down_proj: bfloat16 [32, 2048, 2048], P('sp', 'tp')
- grad_out_proj: float32 [2048, 4096], P('sp', 'tp')
- grad_values: bfloat16 [4096, 4096], P('sp', 'tp')
- grad_gate: bfloat16 [4096, 4096], P('sp', 'tp')
- grad_input_keys: bfloat16 [4096, 2048], P('sp', 'tp')
- grad_output_keys: bfloat16 [4096, 2048], P('sp', 'tp')
- grad_steps: float32 [4096, 64], P('sp', 'tp')
Inputs may be any that keep to these rules, and one draw needn't show every extreme that they name: In the rows of one device no expert is named by more than 12 routes, and on some devices one expert is named by exactly 12; the 2 routes of a token name different experts.
All inputs are finite; a program needn't handle non-finite values.
Results may differ from a plain program's by a relative error of at most 0.025.
Values may be sent and summed in bfloat16 or wider, within the bound.
A program may use at most 64 MiB of HBM per device.

v0:
```python
import jax
import jax.numpy as jnp
from jax import lax
from jax.sharding import Mesh
from jax.sharding import PartitionSpec as P

NSTATE = 128
BLOCK = 128
SP = ("sp_0", "sp_1")


CLAMP_LIMIT = 7.0
SIGMOID_SCALE = 1.702


def side_by_side(arrays, axis, split_dim, concat_dim, along):
    both = jnp.concatenate(arrays, axis=along)
    out, at, gathered = (
        lax.all_to_all(both, axis, split_axis=split_dim, concat_axis=concat_dim, tiled=True),
        0,
        [],
    )
    for a in arrays:
        gathered.append(lax.slice_in_dim(out, at, at + a.shape[along], axis=along))
        at += a.shape[along]
    return tuple(gathered)


def in_blocks(x, dim, count):
    lengths = x.shape
    tiles = x.reshape(*lengths[:dim], count, lengths[dim] // count, *lengths[dim + 1 :])
    return jnp.moveaxis(tiles, dim, 0)


def summed_on_arrival(x, axis, dim):
    tiles = in_blocks(x, dim, lax.axis_size(axis))
    arrived = lax.all_to_all(tiles, axis, split_axis=0, concat_axis=0, tiled=True)
    return arrived.astype(jnp.float32).sum(axis=0)


def filled_with(x, identity):
    return jax.tree.map(
        lambda a, e: jnp.broadcast_to(jnp.asarray(e, a.dtype), a.shape), x, identity
    )


def carried_in(x, axes, combine, identity, reverse):
    before = start = filled_with(x, identity)
    so_far = x
    for axis in reversed(axes):
        count, here = (lax.axis_size(axis), lax.axis_index(axis))
        pieces = jax.tree.map(lambda part: lax.all_gather(part, axis), so_far)
        inside, so_far = (start, start)
        for k in reversed(range(count)) if reverse else range(count):
            passed = k > here if reverse else k < here
            so_far = combine(so_far, jax.tree.map(lambda part: part[k], pieces))
            inside = jax.tree.map(lambda new, old: jnp.where(passed, new, old), so_far, inside)
        before = combine(inside, before)
    return before


def decay_span(head_values, in_keys, out_keys, head_steps, head_rates, start_state):
    length = head_values.shape[0]
    num_blocks = length // BLOCK
    causal_mask = jnp.tril(jnp.ones((BLOCK, BLOCK), dtype=bool))

    def advance(carry_state, block_data):
        block_values, block_in, block_out, block_steps = block_data
        log_decay = jnp.cumsum(-block_steps * head_rates, axis=0)
        weighted = block_values * block_steps[..., None]
        ordered = jnp.transpose(log_decay, (1, 2, 0))
        log_gaps = ordered[..., :, None] - ordered[..., None, :]
        mixing = jnp.where(causal_mask, jnp.exp(jnp.where(causal_mask, log_gaps, 0.0)), 0.0)
        scores = jnp.einsum("lgn,sgn->gls", block_out, block_in)
        within = jnp.einsum("grls,sgrp->lgrp", scores[:, None] * mixing, weighted)
        carried = (
            jnp.einsum("lgn,grpn->lgrp", block_out, carry_state) * jnp.exp(log_decay)[..., None]
        )
        to_end = jnp.exp(log_decay[-1] - log_decay)
        new_state = carry_state * jnp.exp(log_decay[-1])[..., None, None] + jnp.einsum(
            "lgn,lgrp->grpn", block_in, weighted * to_end[..., None]
        )
        return (new_state, within + carried)

    blocks = tuple(
        (
            whole_array.reshape((num_blocks, BLOCK) + whole_array.shape[1:])
            for whole_array in (head_values, in_keys, out_keys, head_steps)
        )
    )
    last_state, block_outputs = lax.scan(advance, start_state, blocks)
    return (block_outputs.reshape(head_values.shape), last_state)


def expert_backward(in_slots, grad_slots, gate_weight, up_weight, down_weight):
    model_width = in_slots.shape[-1]
    in_rows = in_slots.reshape(-1, model_width)
    grad_rows = grad_slots.reshape(-1, model_width)
    contract = (((1,), (1,)), ((), ()))
    across = (((0,), (0,)), ((), ()))
    gate_pre = lax.dot_general(in_rows, gate_weight, contract, preferred_element_type=jnp.float32)
    up_pre = lax.dot_general(in_rows, up_weight, contract, preferred_element_type=jnp.float32)
    gate_clamped = jnp.minimum(gate_pre, CLAMP_LIMIT)
    up_clamped = jnp.clip(up_pre, -CLAMP_LIMIT, CLAMP_LIMIT)
    gate_sigmoid = jax.nn.sigmoid(SIGMOID_SCALE * gate_clamped)
    activation = ((up_clamped + 1.0) * gate_clamped * gate_sigmoid).astype(jnp.bfloat16)
    act_grad = lax.dot_general(grad_rows, down_weight, contract, preferred_element_type=jnp.float32)
    gate_grad = jnp.where(
        gate_pre < CLAMP_LIMIT,
        act_grad
        * (up_clamped + 1.0)
        * gate_sigmoid
        * (1.0 + SIGMOID_SCALE * gate_clamped * (1.0 - gate_sigmoid)),
        0.0,
    ).astype(jnp.bfloat16)
    up_grad = jnp.where(
        jnp.abs(up_pre) < CLAMP_LIMIT, act_grad * gate_clamped * gate_sigmoid, 0.0
    ).astype(jnp.bfloat16)
    grad_down = lax.dot_general(
        activation, grad_rows, across, preferred_element_type=jnp.float32
    ).astype(jnp.bfloat16)
    grad_gate_w = lax.dot_general(
        gate_grad, in_rows, across, preferred_element_type=jnp.float32
    ).astype(jnp.bfloat16)
    grad_up_w = lax.dot_general(
        up_grad, in_rows, across, preferred_element_type=jnp.float32
    ).astype(jnp.bfloat16)
    input_grad = jnp.dot(gate_grad, gate_weight, preferred_element_type=jnp.float32) + jnp.dot(
        up_grad, up_weight, preferred_element_type=jnp.float32
    )
    return (grad_gate_w, grad_up_w, grad_down, input_grad.reshape(in_slots.shape))


def compose(earlier, later):
    return (earlier[0] * later[0], later[0][..., None, None] * earlier[1] + later[1])


def body(
    mix_values,
    mix_gate,
    input_keys,
    output_keys,
    step_sizes,
    decay_rates,
    out_proj,
    expert_inputs,
    stream_grad,
    routes,
    route_weights,
    gate_proj,
    up_proj,
    down_proj,
):
    tok_rows = mix_values.shape[0]
    model_width = stream_grad.shape[1]
    route_count = routes.shape[1]
    sp_devices = lax.axis_size(SP)
    tp_devices = lax.axis_size("tp")
    local_experts = gate_proj.shape[0]
    all_experts = local_experts * sp_devices
    capacity = 3 * tok_rows * route_count // (2 * all_experts)
    num_heads = step_sizes.shape[1]
    num_groups = input_keys.shape[1] // NSTATE
    per_group = num_heads // num_groups
    head_size = mix_values.shape[1] // num_heads
    across = (((0,), (0,)), ((), ()))
    flat_routes = routes.reshape(-1)
    one_hot = (flat_routes[:, None] == jnp.arange(all_experts, dtype=jnp.int32)[None, :]).astype(
        jnp.int32
    )
    slot_rank = jnp.sum((jnp.cumsum(one_hot, axis=0) - 1) * one_hot, axis=1)
    slot_index = flat_routes * capacity + slot_rank
    slot_table = (
        jnp.zeros((all_experts * capacity,), jnp.int32)
        .at[slot_index]
        .set(jnp.arange(tok_rows * route_count, dtype=jnp.int32) + 1)
    )
    slot_used = slot_table > 0
    route_id = jnp.maximum(slot_table - 1, 0)
    token_id = route_id // route_count
    route_scale = jnp.where(slot_used, route_weights.reshape(-1)[route_id], 0.0)
    send_grad = (
        (stream_grad[token_id].astype(jnp.float32) * route_scale[:, None])
        .astype(jnp.bfloat16)
        .reshape(all_experts, capacity, model_width)
    )
    send_rows = jnp.where(
        slot_used[:, None], expert_inputs[token_id], jnp.zeros((), jnp.bfloat16)
    ).reshape(all_experts, capacity, model_width)
    got_grad, got_rows = side_by_side((send_grad, send_rows), SP, 0, 0, 1)
    got_grad = got_grad.reshape(sp_devices, local_experts, capacity, model_width)
    got_rows = got_rows.reshape(sp_devices, local_experts, capacity, model_width)
    grad_gate_proj, grad_up_proj, grad_down_proj, partial_back = jax.vmap(
        expert_backward, in_axes=(1, 1, 0, 0, 0), out_axes=(0, 0, 0, 1)
    )(got_rows, got_grad, gate_proj, up_proj, down_proj)
    col_width = model_width // tp_devices
    column = lax.axis_index("tp")
    stream_cols = lax.dynamic_slice_in_dim(stream_grad, column * col_width, col_width, 1).astype(
        jnp.float32
    )
    reduced = summed_on_arrival(
        partial_back.reshape(all_experts * capacity, model_width).astype(jnp.bfloat16), "tp", 1
    )
    returned = lax.all_to_all(
        reduced.reshape(all_experts, capacity, col_width).astype(jnp.bfloat16),
        SP,
        split_axis=0,
        concat_axis=0,
        tiled=True,
    ).astype(jnp.float32)
    summed = jnp.sum(
        returned.reshape(all_experts * capacity, col_width)[slot_index].reshape(
            tok_rows, route_count, col_width
        ),
        axis=1,
    )
    stream_part = (stream_cols + summed).astype(jnp.bfloat16)
    stream_total = lax.all_gather(stream_part, "tp", axis=1, tiled=True)
    head_values = mix_values.astype(jnp.float32).reshape(tok_rows, num_groups, per_group, head_size)
    in_keys = input_keys.astype(jnp.float32).reshape(tok_rows, num_groups, NSTATE)
    out_keys = output_keys.astype(jnp.float32).reshape(tok_rows, num_groups, NSTATE)
    head_steps = step_sizes.reshape(tok_rows, num_groups, per_group)
    head_rates = decay_rates.reshape(num_groups, per_group)
    zero_state = jnp.zeros((num_groups, per_group, head_size, NSTATE), jnp.float32)

    def local_span(values_in, keys_in, keys_out, steps_in):
        return decay_span(values_in, keys_in, keys_out, steps_in, head_rates, zero_state)

    (own_out, own_state), back_local = jax.vjp(
        local_span, head_values, in_keys, out_keys, head_steps
    )
    span_decay = jnp.exp(-jnp.sum(head_steps * head_rates, axis=0))
    identity = (jnp.ones_like(span_decay), jnp.zeros_like(own_state))
    state_in = carried_in((span_decay, own_state), SP, compose, identity, False)[1]

    def entering(state_value, keys_out, steps_in):
        decay_here = jnp.exp(jnp.cumsum(-steps_in * head_rates, axis=0))
        return jnp.einsum("lgn,grpn->lgrp", keys_out, state_value) * decay_here[..., None]

    enter_out, back_enter = jax.vjp(entering, state_in, out_keys, head_steps)
    mixer_out = own_out + enter_out
    gate_in = mix_gate.astype(jnp.float32).reshape(tok_rows, num_groups, per_group, head_size)
    gate_sigmoid = jax.nn.sigmoid(gate_in)
    gate_silu = gate_in * gate_sigmoid
    gated_out = (mixer_out * gate_silu).reshape(tok_rows, -1).astype(jnp.bfloat16)
    stream_part_cols = stream_total
    gated_grad = jnp.dot(
        stream_part_cols,
        lax.all_gather(out_proj, SP, axis=0, tiled=True),
        preferred_element_type=jnp.float32,
    )
    gated_grad = gated_grad.reshape(tok_rows, num_groups, per_group, head_size)
    grad_gate = (
        (gated_grad * mixer_out * gate_sigmoid * (1.0 + gate_in * (1.0 - gate_sigmoid)))
        .reshape(tok_rows, -1)
        .astype(jnp.bfloat16)
    )
    mixer_grad = gated_grad * gate_silu
    state_grad, keys_grad_enter, steps_grad_enter = back_enter(mixer_grad)
    state_out_grad = carried_in((span_decay, state_grad), SP, compose, identity, True)[1]
    grad_vals, grad_in, keys_grad_own, steps_grad_own = back_local((mixer_grad, state_out_grad))
    decay_grad = -head_rates * span_decay * jnp.sum(state_out_grad * state_in, axis=(2, 3))
    grad_steps = (steps_grad_own + steps_grad_enter + decay_grad[None]).reshape(tok_rows, num_heads)
    stream_part_cols = stream_total
    grad_out_proj = summed_on_arrival(
        lax.dot_general(
            stream_part_cols, gated_out, across, preferred_element_type=jnp.float32
        ).astype(jnp.bfloat16),
        SP,
        0,
    )
    return (
        grad_gate_proj,
        grad_up_proj,
        grad_down_proj,
        grad_out_proj,
        grad_vals.reshape(tok_rows, -1).astype(jnp.bfloat16),
        grad_gate,
        grad_in.reshape(tok_rows, -1).astype(jnp.bfloat16),
        (keys_grad_own + keys_grad_enter).reshape(tok_rows, -1).astype(jnp.bfloat16),
        grad_steps,
    )


def solution(mesh):
    finer = Mesh(mesh.devices.reshape(16, 2, mesh.shape["tp"]), ("sp_0", "sp_1", "tp"))
    in_specs = (
        P(SP, "tp"),
        P(SP, "tp"),
        P(SP, "tp"),
        P(SP, "tp"),
        P(SP, "tp"),
        P("tp"),
        P(SP, "tp"),
        P(SP, None),
        P(SP, None),
        P(SP, None),
        P(SP, None),
        P(SP, "tp", None),
        P(SP, "tp", None),
        P(SP, "tp", None),
    )
    out_specs = (
        P(SP, "tp", None),
        P(SP, "tp", None),
        P(SP, "tp", None),
        P(SP, "tp"),
        P(SP, "tp"),
        P(SP, "tp"),
        P(SP, "tp"),
        P(SP, "tp"),
        P(SP, "tp"),
    )
    return jax.shard_map(body, mesh=finer, in_specs=in_specs, out_specs=out_specs, check_vma=False)
```

profile of v0, /device:TPU:1, one launch (start us, length us, event | category | flops | bytes accessed | tf_op | source)
XLA Modules:
  0.0 438.5 jit_solution(11572446071914704919)
XLA Ops:
  11.7 3.1 gather_fusion.2
  14.8 2.4 gather.17
  17.5 2.8 gather_fusion.1
  20.5 3.1 gather_fusion
  23.6 3.9 reshape.2235
  27.8 2.0 copy-done.3
  30.1 2.6 pad_maximum_fusion
  32.7 16.9 %all-to-all-start = ((bf16[32,24,2048]{2,1,0:T(8,128)(2,1)}), bf16[32,24,2048]{2,1,0:T(8,128)(2,1)}, u32[]{:S(2)}, u32[]{:S(2)}) async-start(bf16[32,24,2048]{2,1,0:T(8,128)(2,1)} %pad_maximum_fusion), calls=%async_computation | async-start | bytes 6291456 | tf_op jit(solution)/shard_map/all_to_all | solution.py:19
  51.9 2.5 all-reduce.2
  58.4 2.0 all-gather.1
  62.3 149.6 %all-to-all-done = bf16[32,24,2048]{2,1,0:T(8,128)(2,1)} async-done(((bf16[32,24,2048]{2,1,0:T(8,128)(2,1)}), bf16[32,24,2048]{2,1,0:T(8,128)(2,1)}, u32[]{:S(2)}, u32[]{:S(2)}) %all-to-all-start) | async-done | bytes 3145760 | tf_op jit(solution)/shard_map/all_to_all | solution.py:19
  211.9 5.4 %fusion.311 = (bf16[32,12,2048]{2,1,0:T(8,128)(2,1)}, bf16[32,12,2048]{2,1,0:T(8,128)(2,1)}) fusion(bf16[32,24,2048]{2,1,0:T(8,128)(2,1)} %all-to-all-done), kind=kLoop, calls=%fused_computation.451 | loop fusion | bytes 6291456 | tf_op jit(solution)/shard_map/slice | solution.py:24
  217.4 2.5 reshape.2219
  219.9 3.7 reshape.2221
  228.5 7.0 %all-to-all-start.1 = ((bf16[16,384,128]{2,1,0:T(8,128)(2,1)}), bf16[16,384,128]{2,1,0:T(8,128)(2,1)}, u32[]{:S(2)}, u32[]{:S(2)}) async-start(bf16[16,384,128]{2,1,0:T(8,128)(2,1)} %bitcast.508), calls=%async_computation.1 | async-start | bytes 3145728 | tf_op jit(solution)/shard_map/all_to_all | solution.py:37
  236.3 24.1 %all-reduce.3 = f32[64]{0:T(128)S(1)} all-reduce(f32[64]{0:T(128)S(1)} %copy-done.96), channel_id=5, replica_groups=mesh['sp_0'=16,'sp_1'=2,'tp'=16] {'sp_0'}, use_global_device_ids=true, to_apply=%add.3 | all-reduce | flops 64 | bytes 512
  265.7 13.1 %all-to-all-start.2 = ((bf16[32,12,128]{2,1,0:T(8,128)(2,1)}), bf16[32,12,128]{2,1,0:T(8,128)(2,1)}, u32[]{:S(2)}, u32[]{:S(2)}) async-start(bf16[32,12,128]{2,1,0:T(8,128)(2,1)} %convert_element_type.124), calls=%async_computation.2 | async-start | bytes 262144 | tf_op jit(solution)/shard_map/all_to_all | solution.py:204
  280.7 2.0 select_add_fusion
  283.7 13.0 %all-to-all-done.2 = bf16[32,12,128]{2,1,0:T(8,128)(2,1)} async-done(((bf16[32,12,128]{2,1,0:T(8,128)(2,1)}), bf16[32,12,128]{2,1,0:T(8,128)(2,1)}, u32[]{:S(2)}, u32[]{:S(2)}) %all-to-all-start.2) | async-done | bytes 98336 | tf_op jit(solution)/shard_map/all_to_all | solution.py:204
  298.5 19.3 %all_gather.38 = bf16[128,2048]{1,0:T(8,128)(2,1)S(1)} all-gather(bf16[128,128]{1,0:T(8,128)(2,1)S(1)} %add_convert_fusion.1), channel_id=1, replica_groups=mesh['sp_0'=16,'sp_1'=2,'tp'=16] {'tp'}, dimensions={1}, use_global_device_ids=true | all-gather | bytes 557056 | tf_op jit(solution)/shard_map/all_gather | solution.py:218
  317.8 1.7 fusion.319
  319.6 2.5 multiply_reduce_fusion.2
  322.3 7.6 %all-gather.2 = f32[8,64,128]{2,1,0:T(8,128)S(1)} all-gather(f32[4,64,128]{2,1,0:T(8,128)S(1)} %fusion.39), channel_id=4, replica_groups=mesh['sp_0'=16,'sp_1'=2,'tp'=16] {'sp_1'}, dimensions={0}, use_global_device_ids=true | all-gather | bytes 393216 | tf_op jit(solution)/shard_map/all_gather | solution.py:52
  332.1 4.7 %all-to-all-start.3 = ((bf16[32,64,256]{2,1,0:T(8,128)(2,1)}), bf16[32,64,256]{2,1,0:T(8,128)(2,1)}, u32[]{:S(2)}, u32[]{:S(2)}) async-start(bf16[32,64,256]{2,1,0:T(8,128)(2,1)} %bitcast.509), calls=%async_computation.3 | async-start | bytes 2097152 | tf_op jit(solution)/shard_map/all_to_all | solution.py:37
  336.9 2.3 fusion
  342.9 1.7 reduce_window_sum.65
  346.8 69.5 %all-gather.12.cloned.1.call-done = f32[16,1,4,64,128]{4,3,2,1,0:T(8,128)} async-done(((f32[1,1,4,64,128]{4,3,2,1,0:T(8,128)}), f32[16,1,4,64,128]{4,3,2,1,0:T(8,128)}) %all-gather.12.cloned.1.call-update) | async-done | bytes 2097168 | tf_op jit(solution)/shard_map/all_gather | solution.py:52
  416.5 2.1 convolution_bitcast_fusion.2
  418.6 2.0 multiply_reduce_fusion.3
  421.4 2.2 convolution_bitcast_fusion.8
  424.9 2.7 fusion.31
  430.0 2.0 convert_reduce_fusion
  (295 shorter events, 40.0 us)
Async XLA Ops:
  7.2 217.0 %copy-start = (bf16[1,128,2048]{2,1,0:T(8,128)(2,1)S(1)}, bf16[1,128,2048]{2,1,0:T(8,128)(2,1)}, u32[]{:S(2)}) copy-start(bf16[1,128,2048]{2,1,0:T(8,128)(2,1)} %param.25) | copy-start | bytes 1572868
  32.7 179.3 %all-to-all-start = ((bf16[32,24,2048]{2,1,0:T(8,128)(2,1)}), bf16[32,24,2048]{2,1,0:T(8,128)(2,1)}, u32[]{:S(2)}, u32[]{:S(2)}) async-start(bf16[32,24,2048]{2,1,0:T(8,128)(2,1)} %pad_maximum_fusion), calls=%async_computation | async-start | bytes 6291456 | tf_op jit(solution)/shard_map/all_to_all | solution.py:19
  49.6 231.1 %all-gather.8.cloned.1.call-start = ((), (), s32[]{:S(2)}) async-start(), calls=%async_computation.4 | async-start | bytes 2228224 | tf_op jit(solution)/shard_map/all_gather | solution.py:52
  61.0 156.4 %copy-start.95 = (f32[64]{0:T(128)}, f32[64]{0:T(128)S(1)}, u32[]{:S(2)}) copy-start(f32[64]{0:T(128)S(1)} %get-tuple-element.415) | copy-start | bytes 772
  228.5 34.9 %all-to-all-start.1 = ((bf16[16,384,128]{2,1,0:T(8,128)(2,1)}), bf16[16,384,128]{2,1,0:T(8,128)(2,1)}, u32[]{:S(2)}, u32[]{:S(2)}) async-start(bf16[16,384,128]{2,1,0:T(8,128)(2,1)} %bitcast.508), calls=%async_computation.1 | async-start | bytes 3145728 | tf_op jit(solution)/shard_map/all_to_all | solution.py:37
  235.5 45.1 %copy-start.42 = (f32[4]{0:T(128)S(1)}, f32[4]{0:T(128)}, u32[]{:S(2)}) copy-start(f32[4]{0:T(128)} %copy-done.41) | copy-start | bytes 52
  235.6 82.2 %all-gather.10.cloned.1.call-start = ((), (), s32[]{:S(2)}) async-start(), calls=%async_computation.5 | async-start | bytes 1081344 | tf_op jit(solution)/shard_map/all_gather | solution.py:249
  265.7 30.9 %all-to-all-start.2 = ((bf16[32,12,128]{2,1,0:T(8,128)(2,1)}), bf16[32,12,128]{2,1,0:T(8,128)(2,1)}, u32[]{:S(2)}, u32[]{:S(2)}) async-start(bf16[32,12,128]{2,1,0:T(8,128)(2,1)} %convert_element_type.124), calls=%async_computation.2 | async-start | bytes 262144 | tf_op jit(solution)/shard_map/all_to_all | solution.py:204
  278.8 137.4 %all-gather.12.cloned.1.call-start = ((), (), s32[]{:S(2)}) async-start(), calls=%async_computation.6 | async-start | bytes 2228224 | tf_op jit(solution)/shard_map/all_gather | solution.py:52
  329.9 86.4 %copy-start.7 = (f32[8,64,128]{2,1,0:T(8,128)}, f32[8,64,128]{2,1,0:T(8,128)S(1)}, u32[]{:S(2)}) copy-start(f32[8,64,128]{2,1,0:T(8,128)S(1)} %all-gather.2) | copy-start | bytes 786436
  332.1 97.9 %all-to-all-start.3 = ((bf16[32,64,256]{2,1,0:T(8,128)(2,1)}), bf16[32,64,256]{2,1,0:T(8,128)(2,1)}, u32[]{:S(2)}, u32[]{:S(2)}) async-start(bf16[32,64,256]{2,1,0:T(8,128)(2,1)} %bitcast.509), calls=%async_computation.3 | async-start | bytes 2097152 | tf_op jit(solution)/shard_map/all_to_all | solution.py:37
  340.6 75.7 %copy-start.48 = (f32[4]{0:T(128)S(1)}, f32[4]{0:T(128)}, u32[]{:S(2)}) copy-start(f32[4]{0:T(128)} %get-tuple-element.413) | copy-start | bytes 52
  340.6 75.7 %copy-start.51 = (f32[4]{0:T(128)S(1)}, f32[4]{0:T(128)}, u32[]{:S(2)}) copy-start(f32[4]{0:T(128)} %get-tuple-element.417) | copy-start | bytes 52
  340.6 75.7 %copy-start.54 = (f32[4]{0:T(128)S(1)}, f32[4]{0:T(128)}, u32[]{:S(2)}) copy-start(f32[4]{0:T(128)} %copy-done.53) | copy-start | bytes 52
  340.6 75.7 %copy-start.56 = (f32[4]{0:T(128)S(1)}, f32[4]{0:T(128)}, u32[]{:S(2)}) copy-start(f32[4]{0:T(128)} %copy-done.55) | copy-start | bytes 52
  340.6 75.7 %copy-start.58 = (f32[4]{0:T(128)S(1)}, f32[4]{0:T(128)}, u32[]{:S(2)}) copy-start(f32[4]{0:T(128)} %copy-done.57) | copy-start | bytes 52
  340.6 75.7 %copy-start.60 = (f32[4]{0:T(128)S(1)}, f32[4]{0:T(128)}, u32[]{:S(2)}) copy-start(f32[4]{0:T(128)} %copy-done.59) | copy-start | bytes 52
  340.6 75.7 %copy-start.62 = (f32[4]{0:T(128)S(1)}, f32[4]{0:T(128)}, u32[]{:S(2)}) copy-start(f32[4]{0:T(128)} %copy-done.61) | copy-start | bytes 52
  340.6 75.7 %copy-start.64 = (f32[4]{0:T(128)S(1)}, f32[4]{0:T(128)}, u32[]{:S(2)}) copy-start(f32[4]{0:T(128)} %copy-done.63) | copy-start | bytes 52
  340.6 75.7 %copy-start.66 = (f32[4]{0:T(128)S(1)}, f32[4]{0:T(128)}, u32[]{:S(2)}) copy-start(f32[4]{0:T(128)} %copy-done.65) | copy-start | bytes 52
  340.6 75.7 %copy-start.68 = (f32[4]{0:T(128)S(1)}, f32[4]{0:T(128)}, u32[]{:S(2)}) copy-start(f32[4]{0:T(128)} %copy-done.67) | copy-start | bytes 52
  340.7 75.7 %copy-start.70 = (f32[4]{0:T(128)S(1)}, f32[4]{0:T(128)}, u32[]{:S(2)}) copy-start(f32[4]{0:T(128)} %copy-done.69) | copy-start | bytes 52
  340.7 75.7 %copy-start.72 = (f32[4]{0:T(128)S(1)}, f32[4]{0:T(128)}, u32[]{:S(2)}) copy-start(f32[4]{0:T(128)} %copy-done.71) | copy-start | bytes 52
  340.7 75.7 %copy-start.74 = (f32[4]{0:T(128)S(1)}, f32[4]{0:T(128)}, u32[]{:S(2)}) copy-start(f32[4]{0:T(128)} %copy-done.73) | copy-start | bytes 52
  340.7 75.7 %copy-start.76 = (f32[4]{0:T(128)S(1)}, f32[4]{0:T(128)}, u32[]{:S(2)}) copy-start(f32[4]{0:T(128)} %copy-done.75) | copy-start | bytes 52
  340.7 75.7 %copy-start.78 = (f32[4]{0:T(128)S(1)}, f32[4]{0:T(128)}, u32[]{:S(2)}) copy-start(f32[4]{0:T(128)} %copy-done.77) | copy-start | bytes 52
  340.7 75.7 %copy-start.81 = (f32[4]{0:T(128)S(1)}, f32[4]{0:T(128)}, u32[]{:S(2)}) copy-start(f32[4]{0:T(128)} %copy-done.80) | copy-start | bytes 52
  340.7 75.7 %copy-start.90 = (f32[4]{0:T(128)S(1)}, f32[4]{0:T(128)}, u32[]{:S(2)}) copy-start(f32[4]{0:T(128)} %get-tuple-element.411) | copy-start | bytes 52
  340.7 75.7 %copy-start.91 = (f32[4]{0:T(128)S(1)}, f32[4]{0:T(128)}, u32[]{:S(2)}) copy-start(f32[4]{0:T(128)} %get-tuple-element.418) | copy-start | bytes 52
  340.7 75.7 %copy-start.92 = (f32[4]{0:T(128)S(1)}, f32[4]{0:T(128)}, u32[]{:S(2)}) copy-start(f32[4]{0:T(128)} %get-tuple-element.419) | copy-start | bytes 52
  346.1 70.2 %copy-start.29 = (bf16[128,128]{1,0:T(8,128)(2,1)}, bf16[128,128]{1,0:T(8,128)(2,1)S(1)}, u32[]{:S(2)}) copy-start(bf16[128,128]{1,0:T(8,128)(2,1)S(1)} %get-tuple-element.388) | copy-start | bytes 98308
  346.1 75.3 %copy-start.18 = (f32[1,1,4,64,128]{4,3,2,1,0:T(8,128)S(1)}, f32[1,1,4,64,128]{4,3,2,1,0:T(8,128)}, u32[]{:S(2)}) copy-start(f32[1,1,4,64,128]{4,3,2,1,0:T(8,128)} %bitcast_add_fusion.52) | copy-start | bytes 393220
  (72 other events, 844.5 us)
Sparse Core Ops, SparseCore 0:
  62.5 137.6 all-gather.7
  238.5 68.6 all-gather.9
  330.7 85.4 all-gather.11
where the time goes:
time: 446 us; the launch traced here: 439 us
  waiting for transfers between devices  233 us (52%)
  blocking collectives  55.4 us (12%)
  local copies, waits for them, and re-layouts  45.5 us (10%)
  starting transfers between devices  42.1 us (9%)
  matrix products  24.8 us (6%)
  other arithmetic  21.6 us (5%)
  between operations  16.5 us (4%)
    all_to_all x1, waiting for transfers between devices, side_by_side(): lax.all_to_all(both, axis, split_axis=split_dim, concat_axis=concat_dim,...  150 us
    all_gather x2, waiting for transfers between devices, carried_in(): pieces = jax.tree.map(lambda part: lax.all_gather(part, axis), so_far)  69.5 us
    unnamed x2, blocking collectives  26.5 us
    all_gather x1, blocking collectives, body(): stream_total = lax.all_gather(stream_part, 'tp', axis=1, tiled=True)  19.3 us
    all_to_all x1, starting transfers between devices, side_by_side(): lax.all_to_all(both, axis, split_axis=split_dim, concat_axis=concat_dim,...  16.9 us
    all_to_all x1, starting transfers between devices, body(): lax.all_to_all(reduced.reshape(all_experts, capacity, col_width).astype(j...  13.1 us
    all_to_all x1, waiting for transfers between devices, body(): lax.all_to_all(reduced.reshape(all_experts, capacity, col_width).astype(j...  13 us
    all_to_all x2, starting transfers between devices, summed_on_arrival(): lax.all_to_all(tiles, axis, split_axis=0, concat_axis=0, tiled=True)  11.7 us
  transfers between devices with their start and end apart: 7, of which 3 were waited for; matrix products, arithmetic and copies ran while one was open for 13% of the time, Pallas kernels for 0%

commit v1 on v0

--- a/solution.py
+++ b/solution.py
@@ -1,12 +1,15 @@
+import functools
+
 import jax
 import jax.numpy as jnp
 from jax import lax
-from jax.sharding import Mesh
+from jax.experimental import pallas as pl
+from jax.experimental.pallas import tpu as pltpu
 from jax.sharding import PartitionSpec as P
 
 NSTATE = 128
 BLOCK = 128
-SP = ("sp_0", "sp_1")
+SP = ("sp",)
 
 
 CLAMP_LIMIT = 7.0
@@ -92,43 +95,467 @@
     return (block_outputs.reshape(head_values.shape), last_state)
 
 
-def expert_backward(in_slots, grad_slots, gate_weight, up_weight, down_weight):
-    model_width = in_slots.shape[-1]
-    in_rows = in_slots.reshape(-1, model_width)
-    grad_rows = grad_slots.reshape(-1, model_width)
-    contract = (((1,), (1,)), ((), ()))
-    across = (((0,), (0,)), ((), ()))
-    gate_pre = lax.dot_general(in_rows, gate_weight, contract, preferred_element_type=jnp.float32)
-    up_pre = lax.dot_general(in_rows, up_weight, contract, preferred_element_type=jnp.float32)
-    gate_clamped = jnp.minimum(gate_pre, CLAMP_LIMIT)
-    up_clamped = jnp.clip(up_pre, -CLAMP_LIMIT, CLAMP_LIMIT)
-    gate_sigmoid = jax.nn.sigmoid(SIGMOID_SCALE * gate_clamped)
-    activation = ((up_clamped + 1.0) * gate_clamped * gate_sigmoid).astype(jnp.bfloat16)
-    act_grad = lax.dot_general(grad_rows, down_weight, contract, preferred_element_type=jnp.float32)
+MESH_ID = pl.DeviceIdType.MESH
+F32 = jnp.float32
+BF16 = jnp.bfloat16
+COLS = 128
+CAP = 12
+RING = 4
+
+
+def nt(a, b):
+    return lax.dot_general(a, b, (((1,), (1,)), ((), ())), preferred_element_type=F32)
+
+
+def tn(a, b):
+    return lax.dot_general(a, b, (((0,), (0,)), ((), ())), preferred_element_type=F32)
+
+
+def nn(a, b):
+    return lax.dot_general(a, b, (((1,), (0,)), ((), ())), preferred_element_type=F32)
+
+
+def iota(shape, dim):
+    return lax.broadcasted_iota(jnp.int32, shape, dim)
+
+
+def up(i, by):
+    return lax.rem(i + by, RING)
+
+
+class Plane:
+    def __init__(self, first_is_x):
+        tp = lax.axis_index("tp")
+        x, y = lax.rem(tp, RING), lax.div(tp, RING)
+        self.first_is_x = first_is_x
+        self.p, self.q = (x, y) if first_is_x else (y, x)
+
+    def tp_of(self, p, q):
+        return q * RING + p if self.first_is_x else p * RING + q
+
+    def at(self, i, j):
+        return self.tp_of(up(self.p, i), up(self.q, j))
+
+
+def remote(src, dst, sems, k, **where):
+    send, recv = sems
+    return pltpu.make_async_remote_copy(
+        src_ref=src,
+        dst_ref=dst,
+        send_sem=send.at[k],
+        recv_sem=recv.at[k],
+        device_id=where,
+        device_id_type=MESH_ID,
+    )
+
+
+class Gather:
+    def __init__(self, plane, buf, row0, rows, sems, base):
+        self.plane, self.buf, self.row0, self.rows, self.sems, self.base = plane, buf, row0, rows, sems, base
+
+    def block(self, tp, part):
+        start, count = self.row0, self.rows
+        if part is not None:
+            count = self.rows // 2
+            start = start + part * count
+        return self.buf.at[pl.ds(start, count), pl.ds(pl.multiple_of(tp * COLS, COLS), COLS)]
+
+    def copy(self, k, i, j, part, di, dj):
+        b = self.block(self.plane.at(i, j), part)
+        return remote(b, b, self.sems, self.base + k, tp=self.plane.at(di, dj))
+
+    def first(self):
+        self.copy(0, 0, 0, None, 1, 0).start()
+        self.copy(1, 0, 0, None, 3, 0).start()
+        self.second(0)
+
+    def second(self, i):
+        n = 4 + 4 * i
+        self.copy(n, i, 0, None, 0, 1).start()
+        self.copy(n + 1, i, 0, None, 0, 3).start()
+
+    def arrived(self, k, i, j, part):
+        self.copy(k, i, j, part, 0, 1).wait_recv()
+
+    def from_low(self):
+        self.arrived(0, 3, 0, None)
+        self.copy(2, 3, 0, 0, 1, 0).start()
+        self.second(3)
+
+    def from_high(self):
+        self.arrived(1, 1, 0, None)
+        self.copy(3, 1, 0, 1, 3, 0).start()
+        self.second(1)
+
+    def opposite(self):
+        self.arrived(2, 2, 0, 0)
+        self.arrived(3, 2, 0, 1)
+        self.second(2)
+
+    def pass_on(self, i):
+        n = 4 + 4 * i
+        self.arrived(n, i, 3, None)
+        self.copy(n + 2, i, 3, 0, 0, 1).start()
+        self.arrived(n + 1, i, 1, None)
+        self.copy(n + 3, i, 1, 1, 0, 3).start()
+
+    def finish(self):
+        for i in (0, 3, 1, 2):
+            n = 4 + 4 * i
+            self.arrived(n + 2, i, 2, 0)
+            self.arrived(n + 3, i, 2, 1)
+        self.copy(0, 0, 0, None, 1, 0).wait_send()
+        self.copy(1, 0, 0, None, 3, 0).wait_send()
+        self.copy(2, 3, 0, 0, 1, 0).wait_send()
+        self.copy(3, 1, 0, 1, 3, 0).wait_send()
+        for i in (0, 3, 1, 2):
+            n = 4 + 4 * i
+            self.copy(n, i, 0, None, 0, 1).wait_send()
+            self.copy(n + 1, i, 0, None, 0, 3).wait_send()
+            self.copy(n + 2, i, 3, 0, 0, 1).wait_send()
+            self.copy(n + 3, i, 1, 1, 0, 3).wait_send()
+
+
+def gather_start(halves):
+    for g in halves:
+        g.first()
+
+
+def gather_rest(halves):
+    for step in ("from_low", "from_high"):
+        for g in halves:
+            getattr(g, step)()
+    for g in halves:
+        g.pass_on(0)
+    for g in halves:
+        g.opposite()
+    for i in (3, 1, 2):
+        for g in halves:
+            g.pass_on(i)
+    for g in halves:
+        g.finish()
+
+
+def split_stage(send, sems, base, bufs, p, to_high, to_low):
+    far_low, far_high, low0, low1, high0, high1, sum_up, sum_down = bufs
+
+    def c(k, src, dst, where):
+        return remote(src, dst, sems, base + k, tp=where)
+
+    sends = [
+        c(0, send(up(p, 2), 0), far_low, to_high),
+        c(1, send(up(p, 2), 1), far_high, to_low),
+        c(2, send(up(p, 1), 1), low1, to_high),
+        c(3, send(up(p, 3), 0), high0, to_low),
+        c(4, sum_up, low0, to_high),
+        c(5, sum_down, high1, to_low),
+    ]
+
+    def start():
+        for k in range(4):
+            sends[k].start()
+
+    def middle():
+        sends[0].wait_recv()
+        sum_up[...] = (far_low[...].astype(F32) + send(up(p, 1), 0)[...].astype(F32)).astype(BF16)
+        sends[4].start()
+        sends[1].wait_recv()
+        sum_down[...] = (far_high[...].astype(F32) + send(up(p, 3), 1)[...].astype(F32)).astype(BF16)
+        sends[5].start()
+
+    def end():
+        for k in (2, 3, 4, 5):
+            sends[k].wait_recv()
+        lower = send(p, 0)[...].astype(F32) + low0[...].astype(F32) + high0[...].astype(F32)
+        upper = send(p, 1)[...].astype(F32) + low1[...].astype(F32) + high1[...].astype(F32)
+        return lower, upper
+
+    def drain():
+        for k in range(6):
+            sends[k].wait_send()
+
+    return start, middle, end, drain
+
+
+def moe_kernel(
+    n_sp,
+    routes_ref,
+    routes_t_ref,
+    route_w_ref,
+    rows_ref,
+    grad_ref,
+    gate_ref,
+    up_ref,
+    down_ref,
+    d_gate_ref,
+    d_up_ref,
+    d_down_ref,
+    total_ref,
+    send1,
+    recv1,
+    all_rows,
+    all_grad,
+    part0,
+    part1,
+    far_a0,
+    far_a1,
+    far_b0,
+    far_b1,
+    mid0,
+    mid1,
+    send2,
+    recv2,
+    s_z1,
+    r_z1,
+    s_ag,
+    r_ag,
+    s_rs,
+    r_rs,
+    s_z2,
+    r_z2,
+    s_tg,
+    r_tg,
+):
+    sp, tp = lax.axis_index("sp"), lax.axis_index("tp")
+    tokens, width = grad_ref.shape
+    slots = n_sp * CAP
+    planes = (Plane(True), Plane(False))
+    barrier = pltpu.get_barrier_semaphore()
+
+    def greet(d, _):
+        pl.semaphore_signal(barrier, inc=1, device_id={"sp": lax.rem(sp + d, n_sp)}, device_id_type=MESH_ID)
+        return 0
+
+    lax.fori_loop(1, n_sp, greet, 0)
+    for i, j in ((1, 0), (3, 0), (0, 1), (0, 3)):
+        pl.semaphore_signal(barrier, inc=1, device_id={"tp": planes[0].at(i, j)}, device_id_type=MESH_ID)
+
+    my_cols = pl.ds(pl.multiple_of(tp * COLS, COLS), COLS)
+    r_row = routes_t_ref[...]
+    expert_rows = iota((n_sp, tokens), 0)
+    hit_t = [(expert_rows == r_row[k : k + 1]) for k in range(2)]
+    any_t = jnp.where(hit_t[0] | hit_t[1], 1.0, 0.0).astype(BF16)
+    before = jnp.where(iota((tokens, tokens), 0) < iota((tokens, tokens), 1), 1.0, 0.0).astype(BF16)
+    ranks_t = nn(any_t, before)
+    rank_row = [
+        jnp.sum(jnp.where(h, ranks_t, 0.0), axis=0, keepdims=True).astype(jnp.int32) for h in hit_t
+    ]
+    e3 = iota((n_sp, 2 * CAP, tokens), 0)
+    c3 = iota((n_sp, 2 * CAP, tokens), 1)
+    here = [
+        [
+            (e3 == r_row[k : k + 1][None]) & (c3 == rank_row[k][None] + shift)
+            for k in range(2)
+        ]
+        for shift in (0, CAP)
+    ]
+
+    def pick(mask):
+        return jnp.where(mask, 1.0, 0.0).reshape(n_sp * 2 * CAP, tokens).astype(BF16)
+
+    cut = here[0][0] | here[0][1]
+    cut = cut & (c3 < CAP)
+    my_grad = grad_ref[:, my_cols].astype(F32)
+    scaled = [(my_grad * route_w_ref[:, k : k + 1]).astype(BF16) for k in range(2)]
+    message = (
+        nn(pick(cut), rows_ref[:, my_cols]) + nn(pick(here[1][0]), scaled[0]) + nn(pick(here[1][1]), scaled[1])
+    )
+    send1[...] = message.astype(BF16).reshape(n_sp, 2 * CAP, COLS)
+
+    pl.semaphore_wait(barrier, n_sp - 1 + 4)
+
+    def z_copy(send, recv, sems, d):
+        to = lax.rem(sp + d, n_sp)
+        return remote(send.at[to], recv.at[sp], sems, d, sp=to)
+
+    def z_start(send, recv, sems):
+        lax.fori_loop(1, n_sp, lambda d, _: (z_copy(send, recv, sems, d).start(), 0)[1], 0)
+        recv[pl.ds(sp, 1)] = send[pl.ds(sp, 1)]
+
+    def z_wait(send, recv, sems):
+        lax.fori_loop(1, n_sp, lambda d, _: (z_copy(send, recv, sems, d).wait(), 0)[1], 0)
+
+    z_start(send1, recv1, (s_z1, r_z1))
+
+    route_cols = routes_ref[...]
+    expert_cols = iota((tokens, n_sp), 1)
+    hit = [(expert_cols == route_cols[:, k : k + 1]) for k in range(2)]
+    any_c = jnp.where(hit[0] | hit[1], 1.0, 0.0).astype(BF16)
+    after = jnp.where(iota((tokens, tokens), 1) < iota((tokens, tokens), 0), 1.0, 0.0).astype(BF16)
+    ranks = nn(after, any_c)
+    j2 = iota((tokens, n_sp * 16), 1)
+    back = None
+    for k in range(2):
+        rank_col = jnp.sum(jnp.where(hit[k], ranks, 0.0), axis=1, keepdims=True).astype(jnp.int32)
+        one = (lax.shift_right_logical(j2, 4) == route_cols[:, k : k + 1]) & ((j2 & 15) == rank_col)
+        back = one if back is None else back | one
+    back = jnp.where(back, 1.0, 0.0).astype(BF16)
+
+    qi, qj = iota((96, 96), 0), iota((96, 96), 1)
+    half = jnp.where(qi >= 48, 1, 0)
+    qr = qi - 48 * half
+    qs = jnp.where(qr >= 36, 3, jnp.where(qr >= 24, 2, jnp.where(qr >= 12, 1, 0)))
+    squeeze = jnp.where(qj == qr + 12 * qs + 12 * half, 1.0, 0.0).astype(BF16)
+
+    z_wait(send1, recv1, (s_z1, r_z1))
+    for g in range(n_sp // 4):
+        got = recv1[pl.ds(4 * g, 4)].reshape(96, COLS)
+        rows = nn(squeeze, got).astype(BF16)
+        all_rows[pl.ds(48 * g, 48), my_cols] = rows[:48]
+        all_grad[pl.ds(48 * g, 48), my_cols] = rows[48:]
+
+    halves = (
+        Gather(planes[0], all_rows, 0, slots, (s_ag, r_ag), 0),
+        Gather(planes[1], all_grad, 0, slots, (s_ag, r_ag), 20),
+    )
+    gather_start(halves)
+    gather_rest(halves)
+
+    x = all_rows[...]
+    g = all_grad[...]
+    gate_pre = nt(x, gate_ref[0])
+    up_pre = nt(x, up_ref[0])
+    act_grad = nt(g, down_ref[0])
+    gate_c = jnp.minimum(gate_pre, CLAMP_LIMIT)
+    up_c = jnp.clip(up_pre, -CLAMP_LIMIT, CLAMP_LIMIT)
+    sg = jax.nn.sigmoid(SIGMOID_SCALE * gate_c)
     gate_grad = jnp.where(
         gate_pre < CLAMP_LIMIT,
-        act_grad
-        * (up_clamped + 1.0)
-        * gate_sigmoid
-        * (1.0 + SIGMOID_SCALE * gate_clamped * (1.0 - gate_sigmoid)),
+        act_grad * (up_c + 1.0) * sg * (1.0 + SIGMOID_SCALE * gate_c * (1.0 - sg)),
         0.0,
-    ).astype(jnp.bfloat16)
-    up_grad = jnp.where(
-        jnp.abs(up_pre) < CLAMP_LIMIT, act_grad * gate_clamped * gate_sigmoid, 0.0
-    ).astype(jnp.bfloat16)
-    grad_down = lax.dot_general(
-        activation, grad_rows, across, preferred_element_type=jnp.float32
-    ).astype(jnp.bfloat16)
-    grad_gate_w = lax.dot_general(
-        gate_grad, in_rows, across, preferred_element_type=jnp.float32
-    ).astype(jnp.bfloat16)
-    grad_up_w = lax.dot_general(
-        up_grad, in_rows, across, preferred_element_type=jnp.float32
-    ).astype(jnp.bfloat16)
-    input_grad = jnp.dot(gate_grad, gate_weight, preferred_element_type=jnp.float32) + jnp.dot(
-        up_grad, up_weight, preferred_element_type=jnp.float32
-    )
-    return (grad_gate_w, grad_up_w, grad_down, input_grad.reshape(in_slots.shape))
+    ).astype(BF16)
+    up_grad = jnp.where(jnp.abs(up_pre) < CLAMP_LIMIT, act_grad * gate_c * sg, 0.0).astype(BF16)
+    activation = ((up_c + 1.0) * gate_c * sg).astype(BF16)
+
+    mid_row = slots // 2
+    for b in range(width // (2 * COLS)):
+        cols = pl.ds(2 * COLS * b, 2 * COLS)
+        part = (nn(gate_grad, gate_ref[0, :, cols]) + nn(up_grad, up_ref[0, :, cols])).astype(BF16)
+        for s in range(2):
+            y, xx = divmod(2 * b + s, RING)
+            piece = part[:, s * COLS : (s + 1) * COLS]
+            part0[xx, y] = piece[:mid_row]
+            part1[y, xx] = piece[mid_row:]
+
+    rs = (s_rs, r_rs)
+    stages = []
+    for h, (plane, part, far) in enumerate(zip(planes, (part0, part1), ((far_a0, far_b0), (far_a1, far_b1)))):
+        stages.append(
+            split_stage(
+                lambda dest, hf, part=part: part.at[dest, pl.ds(2 * hf, 2)],
+                rs,
+                12 * h,
+                [far[0].at[k] for k in range(8)],
+                plane.p,
+                plane.at(1, 0),
+                plane.at(3, 0),
+            )
+        )
+    for st in stages:
+        st[0]()
+    d_down_ref[0] = tn(activation, g).astype(BF16)
+    for st in stages:
+        st[1]()
+    d_gate_ref[0] = tn(gate_grad, x).astype(BF16)
+    second = []
+    for h, (plane, mid, far) in enumerate(zip(planes, (mid0, mid1), (far_b0, far_b1))):
+        lower, upper = stages[h][2]()
+        mid[pl.ds(0, 2)] = lower.astype(BF16)
+        mid[pl.ds(2, 2)] = upper.astype(BF16)
+        quarter = mid_row // 2
+        st = split_stage(
+            lambda dest, hf, mid=mid: mid.at[dest, pl.ds(quarter * hf, quarter)],
+            rs,
+            12 * h + 6,
+            [far.at[k] for k in range(8)],
+            plane.q,
+            plane.at(0, 1),
+            plane.at(0, 3),
+        )
+        st[0]()
+        second.append(st)
+    d_up_ref[0] = tn(up_grad, x).astype(BF16)
+    for st in second:
+        st[1]()
+    ei, ej = iota((64, 48), 0), iota((64, 48), 1)
+    spread = jnp.where(((ei & 15) < CAP) & (ej == lax.shift_right_logical(ei, 4) * CAP + (ei & 15)), 1.0, 0.0)
+    spread = spread.astype(BF16)
+    for h, st in enumerate(second):
+        for hf, piece in enumerate(st[2]()):
+            piece = piece.astype(BF16)
+            for g2 in range(2):
+                at = 4 * (4 * h + 2 * hf + g2)
+                send2[pl.ds(at, 4)] = nn(spread, piece[48 * g2 : 48 * (g2 + 1)]).astype(BF16).reshape(4, 16, COLS)
+
+    z_start(send2, recv2, (s_z2, r_z2))
+    for st in stages + second:
+        st[3]()
+    z_wait(send2, recv2, (s_z2, r_z2))
+    summed = nn(back, recv2[...].reshape(n_sp * 16, COLS))
+    total_ref[:, my_cols] = (my_grad + summed).astype(BF16)
+    rows_half = tokens // 2
+    tg = (s_tg, r_tg)
+    halves = (
+        Gather(planes[0], total_ref, 0, rows_half, tg, 0),
+        Gather(planes[1], total_ref, rows_half, rows_half, tg, 20),
+    )
+    gather_start(halves)
+    gather_rest(halves)
+
+
+def expert_part(routes, route_weights, expert_inputs, stream_grad, gate_proj, up_proj, down_proj):
+    n_sp = lax.axis_size("sp")
+    tokens, width = stream_grad.shape
+    slots = n_sp * CAP
+    n_tp = RING * RING
+    vm = pl.BlockSpec(memory_space=pltpu.VMEM)
+    dma = pltpu.SemaphoreType.DMA
+    w = jax.ShapeDtypeStruct(gate_proj.shape, BF16)
+    return pl.pallas_call(
+        functools.partial(moe_kernel, n_sp),
+        out_shape=(w, w, w, jax.ShapeDtypeStruct((tokens, width), BF16)),
+        in_specs=[vm] * 8,
+        out_specs=(vm,) * 4,
+        scratch_shapes=[
+            pltpu.VMEM((n_sp, 2 * CAP, COLS), BF16),
+            pltpu.VMEM((n_sp, 2 * CAP, COLS), BF16),
+            pltpu.VMEM((slots, width), BF16),
+            pltpu.VMEM((slots, width), BF16),
+            pltpu.VMEM((RING, RING, slots // 2, COLS), BF16),
+            pltpu.VMEM((RING, RING, slots // 2, COLS), BF16),
+            pltpu.VMEM((8, 2, slots // 2, COLS), BF16),
+            pltpu.VMEM((8, 2, slots // 2, COLS), BF16),
+            pltpu.VMEM((8, slots // 4, COLS), BF16),
+            pltpu.VMEM((8, slots // 4, COLS), BF16),
+            pltpu.VMEM((RING, slots // 2, COLS), BF16),
+            pltpu.VMEM((RING, slots // 2, COLS), BF16),
+            pltpu.VMEM((n_sp, 16, COLS), BF16),
+            pltpu.VMEM((n_sp, 16, COLS), BF16),
+            dma((n_sp,)),
+            dma((n_sp,)),
+            dma((40,)),
+            dma((40,)),
+            dma((24,)),
+            dma((24,)),
+            dma((n_sp,)),
+            dma((n_sp,)),
+            dma((40,)),
+            dma((40,)),
+        ],
+        compiler_params=pltpu.CompilerParams(
+            collective_id=0, has_side_effects=True, vmem_limit_bytes=60 * 1024 * 1024
+        ),
+        name="experts",
+    )(
+        routes,
+        routes.T,
+        route_weights,
+        expert_inputs,
+        stream_grad,
+        gate_proj,
+        up_proj,
+        down_proj,
+    )
 
 
 def compose(earlier, later):
@@ -152,70 +579,14 @@
     down_proj,
 ):
     tok_rows = mix_values.shape[0]
-    model_width = stream_grad.shape[1]
-    route_count = routes.shape[1]
-    sp_devices = lax.axis_size(SP)
-    tp_devices = lax.axis_size("tp")
-    local_experts = gate_proj.shape[0]
-    all_experts = local_experts * sp_devices
-    capacity = 3 * tok_rows * route_count // (2 * all_experts)
     num_heads = step_sizes.shape[1]
     num_groups = input_keys.shape[1] // NSTATE
     per_group = num_heads // num_groups
     head_size = mix_values.shape[1] // num_heads
     across = (((0,), (0,)), ((), ()))
-    flat_routes = routes.reshape(-1)
-    one_hot = (flat_routes[:, None] == jnp.arange(all_experts, dtype=jnp.int32)[None, :]).astype(
-        jnp.int32
-    )
-    slot_rank = jnp.sum((jnp.cumsum(one_hot, axis=0) - 1) * one_hot, axis=1)
-    slot_index = flat_routes * capacity + slot_rank
-    slot_table = (
-        jnp.zeros((all_experts * capacity,), jnp.int32)
-        .at[slot_index]
-        .set(jnp.arange(tok_rows * route_count, dtype=jnp.int32) + 1)
-    )
-    slot_used = slot_table > 0
-    route_id = jnp.maximum(slot_table - 1, 0)
-    token_id = route_id // route_count
-    route_scale = jnp.where(slot_used, route_weights.reshape(-1)[route_id], 0.0)
-    send_grad = (
-        (stream_grad[token_id].astype(jnp.float32) * route_scale[:, None])
-        .astype(jnp.bfloat16)
-        .reshape(all_experts, capacity, model_width)
-    )
-    send_rows = jnp.where(
-        slot_used[:, None], expert_inputs[token_id], jnp.zeros((), jnp.bfloat16)
-    ).reshape(all_experts, capacity, model_width)
-    got_grad, got_rows = side_by_side((send_grad, send_rows), SP, 0, 0, 1)
-    got_grad = got_grad.reshape(sp_devices, local_experts, capacity, model_width)
-    got_rows = got_rows.reshape(sp_devices, local_experts, capacity, model_width)
-    grad_gate_proj, grad_up_proj, grad_down_proj, partial_back = jax.vmap(
-        expert_backward, in_axes=(1, 1, 0, 0, 0), out_axes=(0, 0, 0, 1)
-    )(got_rows, got_grad, gate_proj, up_proj, down_proj)
-    col_width = model_width // tp_devices
-    column = lax.axis_index("tp")
-    stream_cols = lax.dynamic_slice_in_dim(stream_grad, column * col_width, col_width, 1).astype(
-        jnp.float32
-    )
-    reduced = summed_on_arrival(
-        partial_back.reshape(all_experts * capacity, model_width).astype(jnp.bfloat16), "tp", 1
-    )
-    returned = lax.all_to_all(
-        reduced.reshape(all_experts, capacity, col_width).astype(jnp.bfloat16),
-        SP,
-        split_axis=0,
-        concat_axis=0,
-        tiled=True,
-    ).astype(jnp.float32)
-    summed = jnp.sum(
-        returned.reshape(all_experts * capacity, col_width)[slot_index].reshape(
-            tok_rows, route_count, col_width
-        ),
-        axis=1,
-    )
-    stream_part = (stream_cols + summed).astype(jnp.bfloat16)
-    stream_total = lax.all_gather(stream_part, "tp", axis=1, tiled=True)
+    grad_gate_proj, grad_up_proj, grad_down_proj, stream_total = expert_part(
+        routes, route_weights, expert_inputs, stream_grad, gate_proj, up_proj, down_proj
+    )
     head_values = mix_values.astype(jnp.float32).reshape(tok_rows, num_groups, per_group, head_size)
     in_keys = input_keys.astype(jnp.float32).reshape(tok_rows, num_groups, NSTATE)
     out_keys = output_keys.astype(jnp.float32).reshape(tok_rows, num_groups, NSTATE)
@@ -283,7 +654,6 @@
 
 
 def solution(mesh):
-    finer = Mesh(mesh.devices.reshape(16, 2, mesh.shape["tp"]), ("sp_0", "sp_1", "tp"))
     in_specs = (
         P(SP, "tp"),
         P(SP, "tp"),
@@ -311,4 +681,4 @@
         P(SP, "tp"),
         P(SP, "tp"),
     )
-    return jax.shard_map(body, mesh=finer, in_specs=in_specs, out_specs=out_specs, check_vma=False)
+    return jax.shard_map(body, mesh=mesh, in_specs=in_specs, out_specs=out_specs, check_vma=False)

time: 446 us -> 295 us (0.66); the launches traced: 439 us -> 294 us
  waiting for transfers between devices: 233 us -> 84.4 us
  Pallas kernels: 0 us -> 98.4 us
  starting transfers between devices: 42.1 us -> 6.22 us
  local copies, waits for them, and re-layouts: 45.5 us -> 13.1 us
  matrix products: 24.8 us -> 14.5 us
  other arithmetic: 21.6 us -> 13.6 us
  blocking collectives: 55.4 us -> 49.2 us
    all_to_all x2 -> x0, waiting for transfers between devices: 163 us -> none  [the longest x1 150 us: side_by_side(): lax.all_to_all(both, axis, split_axis=split_dim, concat_axis=concat_dim,...]
    pallas_call x0 -> x1, Pallas kernels: none -> 98.4 us  [expert_part(): pl.pallas_call(functools.partial(moe_kernel, n_sp), out_shape=(w, w, w, j...]
    all_to_all x2 -> x1, waiting for transfers between devices: 0.01 us -> 62.5 us  [summed_on_arrival(): lax.all_to_all(tiles, axis, split_axis=0, concat_axis=0, tiled=True)]
    all_gather x2, waiting for transfers between devices: 69.5 us -> 21.3 us  [carried_in(): pieces = jax.tree.map(lambda part: lax.all_gather(part, axis), so_far)]
    all_to_all x2 -> x0, starting transfers between devices: 30 us -> none  [the longest x1 16.9 us: side_by_side(): lax.all_to_all(both, axis, split_axis=split_dim, concat_axis=concat_dim,...]
    all_gather x3 -> x0, blocking collectives: 28.8 us -> none  [the longest x1 19.3 us: body(): stream_total = lax.all_gather(stream_part, 'tp', axis=1, tiled=True)]
    unnamed x2 -> x1, blocking collectives: 26.5 us -> 49.2 us
    gather x5 -> x0, local copies, waits for them, and re-layouts: 12.2 us -> none  [the longest x2 5.56 us: body(): expert_inputs[token_id]]
  transfers between devices with their start and end apart: 7 -> 4, of which waited for: 3 -> 2; matrix products, arithmetic and copies ran while one was open for 13% -> 6% of each run, Pallas kernels for 0% -> 33%
where the time goes in v1:
time: 295 us; the launch traced here: 294 us
  Pallas kernels  98.4 us (33%)
  waiting for transfers between devices  84.4 us (29%)
  blocking collectives  49.2 us (17%)
  between operations  14.8 us (5%)
  matrix products  14.5 us (5%)
  other arithmetic  13.6 us (5%)
  local copies, waits for them, and re-layouts  13.1 us (4%)
  starting transfers between devices  6.22 us (2%)
    pallas_call x1, Pallas kernels, expert_part(): pl.pallas_call(functools.partial(moe_kernel, n_sp), out_shape=(w, w, w, j...  98.4 us
    all_to_all x1, waiting for transfers between devices, summed_on_arrival(): lax.all_to_all(tiles, axis, split_axis=0, concat_axis=0, tiled=True)  62.5 us
    unnamed x1, blocking collectives  49.2 us
    all_gather x2, waiting for transfers between devices, carried_in(): pieces = jax.tree.map(lambda part: lax.all_gather(part, axis), so_far)  21.3 us
    unnamed x29, local copies, waits for them, and re-layouts  11.2 us
    dot_general x3, matrix products, advance(): jnp.einsum('lgn,lgrp->grpn', block_in, weighted * to_end[..., None])  7.43 us
    all_to_all x1, starting transfers between devices, summed_on_arrival(): lax.all_to_all(tiles, axis, split_axis=0, concat_axis=0, tiled=True)  6.1 us
  transfers between devices with their start and end apart: 4, of which 2 were waited for; matrix products, arithmetic and copies ran while one was open for 6% of the time, Pallas kernels for 33%

profile of v1, /device:TPU:1, one launch (start us, length us, event | category | flops | bytes accessed | tf_op | source)
XLA Modules:
  0.0 294.3 jit_solution(2607807907048140213)
XLA Ops:
  7.3 0.7 all-gather.7.cloned.1.call-update
  8.0 0.8 copy.123
  8.8 0.7 negate_multiply_fusion
  9.7 1.0 copy.122
  10.9 0.7 bitcast_multiply_fusion
  11.6 1.6 convolution_add_fusion
  13.3 1.4 copy.120.routes_ref
  14.7 1.4 copy.121.route_w_ref
  16.1 0.9 copy.132
  17.4 1.3 dynamic-slice
  19.3 98.4 %experts.1 = (bf16[1,128,2048]{2,1,0:T(8,128)(2,1)}, bf16[1,128,2048]{2,1,0:T(8,128)(2,1)}, bf16[1,128,2048]{2,1,0:T(8,128)(2,1)}, bf16[128,2048]{1,0:T(8,128)(2,1)}) custom-call(s32[128,2]{1,0:T(8,128)} %copy.120.routes_ref, s32[2,128]{1,0:T(2,128)} %bitcast.762, f32[128,2]{1,0:T(8,128)} %copy.121.route_w_ref, bf16[128,2048]{1,0:T(8,128)(2,1)} %rows_ref.1, ...), custom_call_target="tpu_custom_call" | custom-call | tf_op jit(solution)/shard_map/experts/pallas_call | solution.py:514
  118.0 49.2 %all-reduce.2 = f32[128]{0:T(128)S(1)} all-reduce(f32[128]{0:T(128)S(1)} %fusion.421), channel_id=2, replica_groups=mesh['sp'=32,'tp'=16] {'sp'}, use_global_device_ids=true, to_apply=%add.2 | all-reduce | flops 128 | bytes 1024
  167.8 2.0 fusion.440
  169.8 2.9 fusion.30
  173.1 0.8 fusion.20
  174.0 1.5 convolution_convert_fusion
  175.5 6.1 %all-to-all-start = ((bf16[32,64,256]{2,1,0:T(8,128)(2,1)}), bf16[32,64,256]{2,1,0:T(8,128)(2,1)S(1)}, u32[]{:S(2)}, u32[]{:S(2)}) async-start(bf16[32,64,256]{2,1,0:T(8,128)(2,1)} %bitcast.52), calls=%async_computation | async-start | bytes 2097152 | tf_op jit(solution)/shard_map/all_to_all | solution.py:40
  181.7 0.7 copy.143
  182.6 1.1 reduce_window_sum.51
  184.5 0.8 fusion.6
  185.2 62.5 %all-to-all-done = bf16[32,64,256]{2,1,0:T(8,128)(2,1)S(1)} async-done(((bf16[32,64,256]{2,1,0:T(8,128)(2,1)}), bf16[32,64,256]{2,1,0:T(8,128)(2,1)S(1)}, u32[]{:S(2)}, u32[]{:S(2)}) %all-to-all-start) | async-done | bytes 1048608 | tf_op jit(solution)/shard_map/all_to_all | solution.py:40
  247.7 0.8 convert_reduce_fusion
  248.5 21.3 %all-gather.11.cloned.1.call-done = f32[128,64,128]{2,1,0:T(8,128)} async-done(((f32[4,64,128]{2,1,0:T(8,128)}), f32[128,64,128]{2,1,0:T(8,128)}) %all-gather.11.cloned.1.call-update) | async-done | bytes 4194320 | tf_op jit(solution)/shard_map/all_gather | solution.py:55
  269.7 2.9 convolution_bitcast_fusion.2
  272.9 0.7 copy.142
  273.7 3.0 %convolution_bitcast_fusion.8 = f32[128,1,128]{0,2,1:T(8,128)S(1)} fusion(bf16[128,4,64]{0,2,1:T(8,128)(2,1)S(1)} %bitcast.761, f32[128,64,128]{2,1,0:T(8,128)} %all-gather.11.cloned.1.call-done, f32[4]{0:T(128)S(1)} %get-tuple-element.444, f32[4]{0:T(128)S(1)} %get-tuple-element.414, f32[4]{0:T(128)S(1)} %get-tuple-element.415, ...), kind=kOutput, calls=%fused_computation.17 | convolution fusion | flops 11501568 | bytes 4325920 | tf_op jit(solution)/shard_map/transpose(jvp())/while/body/eval_jaxpr/lgn,lgrp->grpn/dot_general | solution.py:83
  276.8 0.7 copy.144
  277.9 5.1 %fusion.17 = (f32[4]{0:T(128)S(1)}, f32[1,4,64,128]{3,2,1,0:T(8,128)S(1)}) fusion(f32[128,64,128]{2,1,0:T(8,128)} %all-gather.9.cloned.1.call-done, f32[4]{0:T(128)S(1)} %get-tuple-element.413, f32[4]{0:T(128)S(1)} %get-tuple-element.430, f32[4]{0:T(128)S(1)} %get-tuple-element.443, f32[4]{0:T(128)S(1)} %get-tuple-element.442, f32[4]{0:T(128)S(1)} %get-tuple-element.441, ...), kind=kLoop, calls=%fused_computation.32 | loop fusion | flops 6291452 | bytes 8520304 | tf_op jit(solution)/shard_map/reduce_sum | solution.py:633
  283.5 1.1 reduce_window_sum.50
  285.3 0.8 copy.154
  286.1 0.8 copy.155
  286.9 0.8 copy.156
  (60 shorter events, 5.1 us)
Async XLA Ops:
  7.2 160.1 %copy-start = (bf16[128,128]{1,0:T(8,128)(2,1)S(1)}, bf16[128,128]{1,0:T(8,128)(2,1)}, u32[]{:S(2)}) copy-start(bf16[128,128]{1,0:T(8,128)(2,1)} %param.17) | copy-start | bytes 98308
  7.2 110.5 %copy-start.6 = (f32[128,4]{0,1:T(4,128)S(1)}, f32[128,4]{0,1:T(4,128)}, u32[]{:S(2)}) copy-start(f32[128,4]{0,1:T(4,128)} %param.18) | copy-start | bytes 6148
  7.2 110.5 %copy-start.7 = (f32[4]{0:T(128)S(1)}, f32[4]{0:T(128)}, u32[]{:S(2)}) copy-start(f32[4]{0:T(128)} %param.19) | copy-start | bytes 52
  7.2 160.4 %copy-start.5 = (bf16[128,128]{1,0:T(8,128)(2,1)S(1)}, bf16[128,128]{1,0:T(8,128)(2,1)}, u32[]{:S(2)}) copy-start(bf16[128,128]{1,0:T(8,128)(2,1)} %param.16) | copy-start | bytes 98308
  7.2 160.5 %all-gather.7.cloned.1.call-start = ((), (), s32[]{:S(2)}) async-start(), calls=%async_computation.1 | async-start | bytes 1081344 | tf_op jit(solution)/shard_map/all_gather | solution.py:620
  8.0 161.8 %all-gather.9.cloned.1.call-start = ((), (), s32[]{:S(2)}) async-start(), calls=%async_computation.2 | async-start | bytes 4325376 | tf_op jit(solution)/shard_map/all_gather | solution.py:55
  13.2 256.5 %all-gather.11.cloned.1.call-start = ((), (), s32[]{:S(2)}) async-start(), calls=%async_computation.3 | async-start | bytes 4325376 | tf_op jit(solution)/shard_map/all_gather | solution.py:55
  167.8 6.2 %copy-start.1 = (bf16[128,2048]{1,0:T(8,128)(2,1)S(1)}, bf16[128,2048]{1,0:T(8,128)(2,1)}, u32[]{:S(2)}) copy-start(bf16[128,2048]{1,0:T(8,128)(2,1)} %get-tuple-element.348) | copy-start | bytes 1572868
  175.5 72.1 %all-to-all-start = ((bf16[32,64,256]{2,1,0:T(8,128)(2,1)}), bf16[32,64,256]{2,1,0:T(8,128)(2,1)S(1)}, u32[]{:S(2)}, u32[]{:S(2)}) async-start(bf16[32,64,256]{2,1,0:T(8,128)(2,1)} %bitcast.52), calls=%async_computation | async-start | bytes 2097152 | tf_op jit(solution)/shard_map/all_to_all | solution.py:40
  277.9 7.5 %copy-start.4 = (bf16[1,128,2048]{2,1,0:T(8,128)(2,1)S(1)}, bf16[1,128,2048]{2,1,0:T(8,128)(2,1)}, u32[]{:S(2)}) copy-start(bf16[1,128,2048]{2,1,0:T(8,128)(2,1)} %get-tuple-element.454) | copy-start | bytes 1572868
  277.9 8.2 %copy-start.3 = (bf16[1,128,2048]{2,1,0:T(8,128)(2,1)S(1)}, bf16[1,128,2048]{2,1,0:T(8,128)(2,1)}, u32[]{:S(2)}) copy-start(bf16[1,128,2048]{2,1,0:T(8,128)(2,1)} %get-tuple-element.455) | copy-start | bytes 1572868
  277.9 9.0 %copy-start.2 = (bf16[1,128,2048]{2,1,0:T(8,128)(2,1)S(1)}, bf16[1,128,2048]{2,1,0:T(8,128)(2,1)}, u32[]{:S(2)}) copy-start(bf16[1,128,2048]{2,1,0:T(8,128)(2,1)} %get-tuple-element.456) | copy-start | bytes 1572868
Sparse Core Ops, SparseCore 0:
  10.2 77.6 all-gather.6
  90.5 70.6 all-gather.8
  174.1 95.5 all-gather.10
